TPU v7x, 32 devices: a whole 2x2x4 slice. The times are simulated.
32 devices in a mesh: grp: 2 (over y), fs: 4 (over z), tp: 4 (over x, core).
Axes of the slice: x: 2, y: 2, z: 4, core: 2. Of those that a mesh axis runs over, the one named last changes fastest.
Arguments:
- tokens: bfloat16 [4096, 2048], P(('grp', 'fs'), 'tp'), parts along dimension 0, may hold values from -16 to 16
- attn_gain: float32 [2048], replicated, may hold values from 0.1 to 1.9
- w_query: bfloat16 [2048, 1024], P('fs', 'tp'), may hold values from -0.125 to 0.125
- w_key: bfloat16 [2048, 1024], P('fs', 'tp'), may hold values from -0.125 to 0.125
- w_value: bfloat16 [2048, 2048], P('fs', 'tp'), may hold values from -0.125 to 0.125
- w_low: bfloat16 [2048, 32], replicated, may hold values from -0.125 to 0.125
- w_lift: bfloat16 [32, 1024], P(None, 'tp'), may hold values from -1 to 1
- decay_bias: float32 [1024], P('tp'), may hold values from -0.5 to 6
- head_gain: float32 [256], replicated, may hold values from 0.1 to 1.9
- w_out: bfloat16 [2048, 2048], P('tp', 'fs'), may hold values from -0.125 to 0.125
- ffn_gain: float32 [2048], replicated, may hold values from 0.1 to 1.9
- w_gate: bfloat16 [2048, 5632], P('fs', 'tp'), may hold values from -0.125 to 0.125
- w_up: bfloat16 [2048, 5632], P('fs', 'tp'), may hold values from -0.125 to 0.125
- w_down: bfloat16 [5632, 2048], P('tp', 'fs'), may hold values from -0.078125 to 0.078125
- final_gain: float32 [2048], P('tp'), may hold values from 0.1 to 1.9
Outputs:
- result: bfloat16 [4096, 2048], P(('grp', 'fs'), 'tp'), parts along dimension 0
There are 2 independent parts, one for each index of `grp`. A program takes and returns all parts, laid end to end along the dimension named above; an argument that names none is the same for every part. Nothing has to cross between parts.
All inputs are finite; a program needn't handle non-finite values.
Results may differ from a plain program's by a relative error of at most 0.015.
Values may be sent and summed in bfloat16 or wider, within the bound.
A program may use at most 64 MiB of HBM per device.

v0:
```python
import jax
import jax.numpy as jnp
from jax import lax
from jax.sharding import PartitionSpec as P

D = 2048
DK = 128
DV = 256
BLOCK = 64


epsilon = 1e-06
highest = lax.Precision.HIGHEST


def rms_rows(values, gain):
    values = values.astype(jnp.float32)
    factor = lax.rsqrt(jnp.mean(values * values, axis=-1, keepdims=True) + epsilon)
    return values * factor * gain


def blockwise_gla(query_rows, key_rows, value_rows, log_decay, head_count):
    length = query_rows.shape[0]
    blocks = length // BLOCK

    def split_heads(array, depth):
        return (
            array.astype(jnp.float32)
            .reshape(blocks, BLOCK, head_count, depth)
            .transpose(2, 0, 1, 3)
        )

    query_f = split_heads(query_rows, DK) * DK ** (-0.5)
    key_f = split_heads(key_rows, DK)
    value_f = split_heads(value_rows, DV)
    log_cum = jnp.cumsum(split_heads(log_decay, DK), axis=2)
    log_last = log_cum[:, :, -1:, :]
    query_dec = query_f * jnp.exp(log_cum)
    key_dec = key_f * jnp.exp(-log_cum)
    causal = jnp.tril(jnp.ones((BLOCK, BLOCK), dtype=bool))
    scores = jnp.where(
        causal, jnp.einsum("hncd,hnsd->hncs", query_dec, key_dec, precision=highest), 0.0
    )
    inside = jnp.einsum("hncs,hnsv->hncv", scores, value_f, precision=highest)
    contrib = jnp.einsum(
        "hncd,hncv->hndv", key_f * jnp.exp(log_last - log_cum), value_f, precision=highest
    )
    decay_block = jnp.exp(log_last[:, :, 0, :])

    def advance(carry_state, inputs):
        decay_step, added = inputs
        return (decay_step[..., None] * carry_state + added, carry_state)

    start_state = jnp.zeros((head_count, DK, DV), jnp.float32)
    final_state, earlier = lax.scan(
        advance, start_state, (jnp.moveaxis(decay_block, 1, 0), jnp.moveaxis(contrib, 1, 0))
    )
    earlier = jnp.moveaxis(earlier, 0, 1)
    output = inside + jnp.einsum("hncd,hndv->hncv", query_dec, earlier, precision=highest)
    return output.transpose(1, 2, 0, 3).reshape(length, head_count, DV)


def body(
    tokens,
    attn_gain,
    w_query,
    w_key,
    w_value,
    w_low,
    w_lift,
    decay_bias,
    head_gain,
    w_out,
    ffn_gain,
    w_gate,
    w_up,
    w_down,
    final_gain,
):
    own_width = tokens.shape[1]
    row_count = tokens.shape[0]
    whole_rows = lax.all_gather(tokens, "tp", axis=1, tiled=True)
    normed = rms_rows(whole_rows, attn_gain).astype(jnp.bfloat16)

    def add_pieces(source, pieces):
        return tuple(
            (
                jnp.dot(source, weight_piece, preferred_element_type=jnp.float32)
                for weight_piece in pieces
            )
        )

    query_sum, key_sum, value_sum = add_pieces(
        normed,
        (
            lax.all_gather(w_query, "fs", axis=0, tiled=True),
            lax.all_gather(w_key, "fs", axis=0, tiled=True),
            lax.all_gather(w_value, "fs", axis=0, tiled=True),
        ),
    )
    query_rows = query_sum.astype(jnp.bfloat16)
    key_rows = key_sum.astype(jnp.bfloat16)
    value_rows = value_sum.astype(jnp.bfloat16)
    low_rank = jnp.dot(normed, w_low, preferred_element_type=jnp.float32).astype(jnp.bfloat16)
    log_decay = (
        jax.nn.log_sigmoid(
            jnp.dot(low_rank, w_lift, preferred_element_type=jnp.float32) + decay_bias
        )
        / 16.0
    )
    head_count = query_rows.shape[1] // DK
    gla_out = blockwise_gla(query_rows, key_rows, value_rows, log_decay, head_count)
    mixed_heads = (
        rms_rows(gla_out, head_gain).reshape(row_count, head_count * DV).astype(jnp.bfloat16)
    )
    out_terms = jnp.dot(
        mixed_heads,
        lax.all_gather(w_out, "fs", axis=1, tiled=True),
        preferred_element_type=jnp.float32,
    )
    total_sum = lax.psum(out_terms.astype(jnp.bfloat16), "tp").astype(jnp.float32)
    full_rows = (whole_rows.astype(jnp.float32) + total_sum).astype(jnp.bfloat16)
    first_sum = lax.dynamic_slice_in_dim(full_rows, lax.axis_index("tp") * own_width, own_width, 1)
    normed_ffn = rms_rows(full_rows, ffn_gain).astype(jnp.bfloat16)
    gate_rows, up_rows = add_pieces(
        normed_ffn,
        (
            lax.all_gather(w_gate, "fs", axis=0, tiled=True),
            lax.all_gather(w_up, "fs", axis=0, tiled=True),
        ),
    )
    hidden = (jax.nn.silu(gate_rows) * up_rows).astype(jnp.bfloat16)
    down_terms = jnp.dot(
        hidden, lax.all_gather(w_down, "fs", axis=1, tiled=True), preferred_element_type=jnp.float32
    )
    own_ffn = lax.psum_scatter(
        down_terms.astype(jnp.bfloat16), "tp", scatter_dimension=1, tiled=True
    ).astype(jnp.float32)
    second_sum = first_sum.astype(jnp.float32) + own_ffn
    square_sum = lax.psum(jnp.sum(second_sum * second_sum, axis=1), "tp")
    factor = lax.rsqrt(square_sum / D + epsilon)[:, None]
    return (second_sum * factor * final_gain).astype(jnp.bfloat16)


def solution(mesh):
    return jax.shard_map(
        body,
        mesh=mesh,
        in_specs=(
            P(("grp", "fs"), "tp"),
            P(),
            P("fs", "tp"),
            P("fs", "tp"),
            P("fs", "tp"),
            P(),
            P(None, "tp"),
            P("tp"),
            P(),
            P("tp", "fs"),
            P(),
            P("fs", "tp"),
            P("fs", "tp"),
            P("tp", "fs"),
            P("tp"),
        ),
        out_specs=P(("grp", "fs"), "tp"),
        check_vma=False,
    )
```

profile of v0, /device:TPU:0, one launch (start us, length us, event | category | flops | bytes accessed | tf_op | source)
XLA Modules:
  0.0 620.5 jit_solution(5567289836711899672)
XLA Ops:
  10.6 23.6 %all-gather.9.cloned.1.call-done = bf16[512,2048]{1,0:T(8,128)(2,1)} async-done(((bf16[512,512]{1,0:T(8,128)(2,1)}), bf16[512,2048]{1,0:T(8,128)(2,1)}) %all-gather.9.cloned.1.call-update) | async-done | bytes 2097168 | tf_op jit(solution)/shard_map/all_gather | solution.py:82
  34.2 2.2 fusion.3
  40.5 23.3 %all-gather.11.cloned.1.call-done = bf16[2048,256]{1,0:T(8,128)(2,1)} async-done(((bf16[512,256]{1,0:T(8,128)(2,1)}), bf16[2048,256]{1,0:T(8,128)(2,1)}) %all-gather.11.cloned.1.call-update) | async-done | bytes 1048592 | tf_op jit(solution)/shard_map/all_gather | solution.py:96
  63.8 2.0 fusion.13
  66.9 25.9 %all-gather.13.cloned.1.call-done = bf16[2048,256]{1,0:T(8,128)(2,1)} async-done(((bf16[512,256]{1,0:T(8,128)(2,1)}), bf16[2048,256]{1,0:T(8,128)(2,1)}) %all-gather.13.cloned.1.call-update) | async-done | bytes 1048592 | tf_op jit(solution)/shard_map/all_gather | solution.py:97
  95.8 43.4 %all-gather.15.cloned.1.call-done = bf16[2048,512]{1,0:T(8,128)(2,1)} async-done(((bf16[512,512]{1,0:T(8,128)(2,1)}), bf16[2048,512]{1,0:T(8,128)(2,1)}) %all-gather.15.cloned.1.call-update) | async-done | bytes 2097168 | tf_op jit(solution)/shard_map/all_gather | solution.py:98
  139.3 2.9 convolution_convert_fusion.2
  142.3 2.8 bitcast_multiply_fusion.1
  145.2 2.4 convolution_bitcast_fusion
  147.5 20.2 %while.13 = (s32[]{:T(128)}, f32[2,128,256]{2,1,0:T(8,128)S(1)}, f32[8,2,128,256]{3,2,1,0:T(8,128)}, f32[8,2,128]{2,0,1:T(8,128)}, f32[8,2,128,256]{3,2,1,0:T(8,128)}, /*index=5*/s32[]{:T(128)}, s32[]{:T(128)}) while((s32[]{:T(128)}, f32[2,128,256]{2,1,0:T(8,128)S(1)}, f32[8,2,128,256]{3,2,1,0:T(8,128)}, f32[8,2,128]{2,0,1:T(8,128)}, ...), condition=%wide.region_3.4_spmd.clone, body=%wide.region_2.3_spmd.clone.sunk | while | flops 262147 | bytes 1314400 | solution.py:55
  167.7 2.1 convolution_select_fusion
  169.8 2.9 fusion.8
  178.1 7.1 %all-gather.17.cloned.1.call-done = bf16[512,2048]{1,0:T(8,128)(2,1)} async-done(((bf16[512,512]{1,0:T(8,128)(2,1)}), bf16[512,2048]{1,0:T(8,128)(2,1)}) %all-gather.17.cloned.1.call-update) | async-done | bytes 2097168 | tf_op jit(solution)/shard_map/all_gather | solution.py:118
  185.2 4.5 convolution_convert_fusion
  192.3 47.8 %all-reduce.2.cloned.1.call-done = bf16[512,2048]{1,0:T(8,128)(2,1)} async-done(((bf16[512,2048]{1,0:T(8,128)(2,1)}), bf16[512,2048]{1,0:T(8,128)(2,1)}) %all-reduce.2.cloned.1.call-update) | async-done | bytes 2097168 | tf_op jit(solution)/shard_map/psum | solution.py:121
  240.1 3.9 fusion
  244.0 104.4 %all-gather.19.cloned.1.call-done = bf16[2048,1408]{1,0:T(8,128)(2,1)} async-done(((bf16[512,1408]{1,0:T(8,128)(2,1)}), bf16[2048,1408]{1,0:T(8,128)(2,1)}) %all-gather.19.cloned.1.call-update) | async-done | bytes 5767184 | tf_op jit(solution)/shard_map/all_gather | solution.py:128
  348.4 8.5 %fusion.17 = f32[512,1408]{1,0:T(8,128)} fusion(bf16[2048,1408]{1,0:T(8,128)(2,1)} %all-gather.19.cloned.1.call-done, bf16[512,2048]{1,0:T(8,128)(2,1)} %get-tuple-element.77, f32[2048]{0:T(1024)S(1)} %copy-done.14, f32[512]{0:T(512)S(1)} %add_rsqrt_fusion.2), kind=kOutput, calls=%fused_computation.40 | convolution fusion | flops 2956984320 | bytes 10758144 | tf_op jit(solution)/shard_map/dot_general | solution.py:88
  356.9 98.1 %all-gather.21.cloned.1.call-done = bf16[2048,1408]{1,0:T(8,128)(2,1)} async-done(((bf16[512,1408]{1,0:T(8,128)(2,1)}), bf16[2048,1408]{1,0:T(8,128)(2,1)}) %all-gather.21.cloned.1.call-update) | async-done | bytes 5767184 | tf_op jit(solution)/shard_map/all_gather | solution.py:129
  455.0 106.5 %all-gather.23.cloned.1.call-done = bf16[1408,2048]{1,0:T(8,128)(2,1)} async-done(((bf16[1408,512]{1,0:T(8,128)(2,1)}), bf16[1408,2048]{1,0:T(8,128)(2,1)}) %all-gather.23.cloned.1.call-update) | async-done | bytes 5767184 | tf_op jit(solution)/shard_map/all_gather | solution.py:134
  561.5 13.4 %convolution_convert_fusion.1 = bf16[512,2048]{1,0:T(8,128)(2,1)} fusion(bf16[1408,2048]{1,0:T(8,128)(2,1)} %all-gather.23.cloned.1.call-done, bf16[2048,1408]{1,0:T(8,128)(2,1)} %all-gather.21.cloned.1.call-done, f32[512,1408]{1,0:T(8,128)} %fusion.17, bf16[512,2048]{1,0:T(8,128)(2,1)S(1)} %copy-done.2, f32[2048]{0:T(1024)S(1)} %copy-done.14, ...), kind=kOutput, calls=%fused_computation.18 | convolution fusion | flops 5915148288 | bytes 18622464 | tf_op jit(solution)/shard_map/dot_general | solution.py:133
  575.0 29.6 %reduce-scatter.2.cloned.1.call-done = bf16[512,512]{1,0:T(8,128)(2,1)} async-done(((bf16[512,2048]{1,0:T(8,128)(2,1)}), bf16[512,512]{1,0:T(8,128)(2,1)}) %reduce-scatter.2.cloned.1.call-update) | async-done | bytes 524304 | tf_op jit(solution)/shard_map/reduce_scatter | solution.py:136
  605.8 5.8 psum.15
  611.6 2.0 multiply_convert_fusion
  (101 shorter events, 41.3 us)
Async XLA Ops:
  6.5 30.5 %copy-start = (bf16[2048,32]{0,1:T(8,128)(2,1)S(1)}, bf16[2048,32]{0,1:T(8,128)(2,1)}, u32[]{:S(2)}) copy-start(bf16[2048,32]{0,1:T(8,128)(2,1)} %param.22) | copy-start | bytes 393220
  6.5 3.5 copy-start.10
  6.5 30.5 %copy-start.11 = (bf16[32,256]{1,0:T(8,128)(2,1)S(1)}, bf16[32,256]{1,0:T(8,128)(2,1)}, u32[]{:S(2)}) copy-start(bf16[32,256]{1,0:T(8,128)(2,1)} %param.23) | copy-start | bytes 49156
  6.5 30.5 %copy-start.12 = (f32[2048]{0:T(1024)S(1)}, f32[2048]{0:T(1024)}, u32[]{:S(2)}) copy-start(f32[2048]{0:T(1024)} %param.18) | copy-start | bytes 24580
  6.5 30.5 %copy-start.15 = (f32[256]{0:T(256)S(1)}, f32[256]{0:T(256)}, u32[]{:S(2)}) copy-start(f32[256]{0:T(256)} %param.24) | copy-start | bytes 3076
  6.5 27.7 %all-gather.9.cloned.1.call-start = ((), (), s32[]{:S(2)}) async-start(), calls=%async_computation.1 | async-start | bytes 2621440 | tf_op jit(solution)/shard_map/all_gather | solution.py:82
  7.3 56.5 %all-gather.11.cloned.1.call-start = ((), (), s32[]{:S(2)}) async-start(), calls=%async_computation.2 | async-start | bytes 1310720 | tf_op jit(solution)/shard_map/all_gather | solution.py:96
  8.0 84.8 %all-gather.13.cloned.1.call-start = ((), (), s32[]{:S(2)}) async-start(), calls=%async_computation.3 | async-start | bytes 1310720 | tf_op jit(solution)/shard_map/all_gather | solution.py:97
  8.8 130.5 %all-gather.15.cloned.1.call-start = ((), (), s32[]{:S(2)}) async-start(), calls=%async_computation.4 | async-start | bytes 2621440 | tf_op jit(solution)/shard_map/all_gather | solution.py:98
  9.3 175.8 %all-gather.17.cloned.1.call-start = ((), (), s32[]{:S(2)}) async-start(), calls=%async_computation.5 | async-start | bytes 2621440 | tf_op jit(solution)/shard_map/all_gather | solution.py:118
  9.9 230.1 %all-reduce.2.cloned.1.call-start = ((), (), s32[]{:S(2)}) async-start(), calls=%async_computation.6 | async-start | bytes 4194304 | tf_op jit(solution)/shard_map/psum | solution.py:121
  34.2 2.8 copy-start.1
  40.5 52.3 %copy-start.9 = (f32[512]{0:T(512)S(1)}, f32[512]{0:T(512)}, u32[]{:S(2)}) copy-start(f32[512]{0:T(512)} %copy-done.8) | copy-start | bytes 6148
  40.5 52.3 %copy-start.13 = (f32[2048]{0:T(1024)S(1)}, f32[2048]{0:T(1024)}, u32[]{:S(2)}) copy-start(f32[2048]{0:T(1024)} %param.18) | copy-start | bytes 24580
  174.4 1.8 copy-start.3
  176.2 9.0 %copy-start.7 = (f32[1,2,2,128]{3,1,2,0:T(2,128)S(1)}, f32[1,2,2,128]{3,1,2,0:T(2,128)}, u32[]{:S(2)}) copy-start(f32[1,2,2,128]{3,1,2,0:T(2,128)} %copy.49) | copy-start | bytes 6148
  177.0 8.2 %copy-start.5 = (f32[64,8,2,256]{3,1,2,0:T(8,128)S(1)}, f32[64,8,2,256]{3,1,2,0:T(8,128)}, u32[]{:S(2)}) copy-start(f32[64,8,2,256]{3,1,2,0:T(8,128)} %copy.48) | copy-start | bytes 3145732
  189.7 158.7 %all-gather.19.cloned.1.call-start = ((), (), s32[]{:S(2)}) async-start(), calls=%async_computation.7 | async-start | bytes 7208960 | tf_op jit(solution)/shard_map/all_gather | solution.py:128
  190.5 264.5 %all-gather.21.cloned.1.call-start = ((), (), s32[]{:S(2)}) async-start(), calls=%async_computation.8 | async-start | bytes 7208960 | tf_op jit(solution)/shard_map/all_gather | solution.py:129
  191.2 370.3 %all-gather.23.cloned.1.call-start = ((), (), s32[]{:S(2)}) async-start(), calls=%async_computation.9 | async-start | bytes 7208960 | tf_op jit(solution)/shard_map/all_gather | solution.py:134
  192.0 156.5 %copy-start.14 = (f32[2048]{0:T(1024)S(1)}, f32[2048]{0:T(1024)}, u32[]{:S(2)}) copy-start(f32[2048]{0:T(1024)} %param.27) | copy-start | bytes 24580
  192.0 412.6 %reduce-scatter.2.cloned.1.call-start = ((), (), s32[]{:S(2)}) async-start(), calls=%async_computation.10 | async-start | bytes 2621440 | tf_op jit(solution)/shard_map/reduce_scatter | solution.py:136
  348.4 213.1 %copy-start.2 = (bf16[512,2048]{1,0:T(8,128)(2,1)S(1)}, bf16[512,2048]{1,0:T(8,128)(2,1)}, u32[]{:S(2)}) copy-start(bf16[512,2048]{1,0:T(8,128)(2,1)} %get-tuple-element.77) | copy-start | bytes 6291460
  574.9 36.7 %copy-start.6 = (f32[512]{0:T(512)S(1)}, f32[512]{0:T(512)}, u32[]{:S(2)}) copy-start(f32[512]{0:T(512)} %param.31) | copy-start | bytes 6148
  (2 other events, 1.3 us)
Sparse Core Ops, SparseCore 0:
  8.9 25.2 all-gather.8
  35.8 27.9 all-gather.10
  65.4 27.3 all-gather.12
  94.2 45.0 all-gather.14
  140.7 44.4 all-gather.16
  189.9 50.1 all-reduce.1
  241.6 106.7 all-gather.18
  350.0 104.9 all-gather.20
  456.6 104.9 all-gather.22
  575.1 29.4 reduce-scatter.1
where the time goes:
time: 622 us; the launch traced here: 621 us
  waiting for transfers between devices  515 us (83%)
  matrix products  43.5 us (7%)
  other arithmetic  27.3 us (4%)
  local copies, waits for them, and re-layouts  14.3 us (2%)
  between operations  13.7 us (2%)
    all_gather x1, waiting for transfers between devices, body(): lax.all_gather(w_down, 'fs', axis=1, tiled=True)  107 us
    all_gather x1, waiting for transfers between devices, body(): lax.all_gather(w_gate, 'fs', axis=0, tiled=True)  104 us
    all_gather x1, waiting for transfers between devices, body(): lax.all_gather(w_up, 'fs', axis=0, tiled=True)  98.1 us
    psum x1, waiting for transfers between devices, body(): lax.psum(out_terms.astype(jnp.bfloat16), 'tp').astype(jnp.float32)  47.8 us
    all_gather x1, waiting for transfers between devices, body(): lax.all_gather(w_value, 'fs', axis=0, tiled=True)  43.4 us
    reduce_scatter x1, waiting for transfers between devices, body(): lax.psum_scatter(down_terms.astype(jnp.bfloat16), 'tp', scatter_dimension...  29.6 us
    all_gather x1, waiting for transfers between devices, body(): lax.all_gather(w_key, 'fs', axis=0, tiled=True)  25.9 us
    all_gather x1, waiting for transfers between devices, body(): whole_rows = lax.all_gather(tokens, 'tp', axis=1, tiled=True)  23.6 us
  transfers between devices with their start and end apart: 10, of which 10 were waited for; matrix products, arithmetic and copies ran while one was open for 10% of the time, Pallas kernels for 0%

commit v1 on v0

v1 whole, which is shorter than its diff:
```python
import functools

import jax
import jax.numpy as jnp
from jax import lax
from jax.experimental import pallas as pl
from jax.experimental.pallas import tpu as pltpu
from jax.sharding import PartitionSpec as P

DK = 128
DV = 256
BLOCK = 64
epsilon = 1e-06
highest = lax.Precision.HIGHEST
MESH = pl.DeviceIdType.MESH
DOWN_CHUNKS = 2


def layer_kernel(
    sizes,
    tokens_ref,
    attn_gain_ref,
    w_low_ref,
    w_lift_ref,
    decay_bias_ref,
    head_gain_ref,
    ffn_gain_ref,
    final_gain_ref,
    w_mix_ref,
    w_out_ref,
    w_gate_ref,
    w_up_ref,
    w_down_ref,
    result_ref,
    g_mix,
    g_out,
    g_gate,
    g_up,
    g_down,
    rows_all,
    normed,
    mix_rows,
    log_decay,
    mixed,
    state,
    partial_out,
    heard_out,
    first_all,
    gate_acc,
    up_acc,
    hidden,
    partial_down,
    heard_down,
    squares,
    z_send,
    z_recv,
    y_send,
    y_recv,
    tp_send,
    tp_recv,
    local_sem,
):
    n, tp = sizes
    g, f, t = lax.axis_index("grp"), lax.axis_index("fs"), lax.axis_index("tp")
    rows, width = tokens_ref.shape
    features = width * tp
    f32 = jnp.float32

    weights = [(w_mix_ref, g_mix), (w_out_ref, g_out), (w_gate_ref, g_gate), (w_up_ref, g_up)]
    messages = [(w, held, 0, 1) for w, held in weights]
    messages += [(w_down_ref, g_down, c, DOWN_CHUNKS) for c in range(DOWN_CHUNKS)]

    barrier = pltpu.get_barrier_semaphore()

    @pl.when(f > 0)
    def _():
        pl.semaphore_signal(barrier, inc=1, device_id=(g, f - 1, t), device_id_type=MESH)

    @pl.when(f < n - 1)
    def _():
        pl.semaphore_signal(barrier, inc=1, device_id=(g, f + 1, t), device_id_type=MESH)

    pl.semaphore_signal(barrier, inc=1, device_id=(1 - g, f, t), device_id_type=MESH)
    for d in range(1, tp):
        peer = lax.rem(t + d, tp)
        pl.semaphore_signal(barrier, inc=1, device_id=(g, f, peer), device_id_type=MESH)
    met = jnp.where(f > 0, 1, 0) + jnp.where(f < n - 1, 1, 0) + tp
    pl.semaphore_wait(barrier, met)

    def span(m, group):
        w, _, chunk, chunks = messages[m]
        part = w.shape[0] // 2
        length = part // chunks
        return pl.ds(pl.multiple_of(group * part + chunk * length, 16), length)

    def z_copy(m, way, step):
        w, held, _, _ = messages[m]
        owner = f - (step - 1) if way == 0 else f + (step - 1)
        at = held.at[owner, span(m, g)]
        source = w.at[span(m, g)] if step == 1 else at
        target = f + 1 if way == 0 else f - 1
        return pltpu.make_async_remote_copy(
            source, at, z_send.at[m, way, step], z_recv.at[m, way, step],
            device_id=(g, target, t), device_id_type=MESH,
        )

    def y_copy(m, way, step):
        held = messages[m][1]
        owner = f - step if way == 0 else f + step
        at = held.at[owner, span(m, g)]
        return pltpu.make_async_remote_copy(
            at, at, y_send.at[m, way, step], y_recv.at[m, way, step],
            device_id=(1 - g, f, t), device_id_type=MESH,
        )

    def gets(way, step):
        return f >= step if way == 0 else f + step < n

    def gives(way, step):
        if way == 0:
            return jnp.logical_and(f + 1 < n, f >= step - 1)
        return jnp.logical_and(f >= 1, f + step - 1 < n)

    def launch(m):
        for way in (0, 1):
            @pl.when(gives(way, 1))
            def _():
                z_copy(m, way, 1).start()

    def tick(m, step):
        for way in (0, 1):
            @pl.when(gets(way, step))
            def _():
                z_copy(m, way, step).wait_recv()
                y_copy(m, way, step).start()

            if step < n - 1:
                @pl.when(gives(way, step + 1))
                def _():
                    z_copy(m, way, step + 1).start()

    def arrived(m, way, step):
        y_copy(m, way, step).wait_recv()

    def all_arrived(m):
        for step in range(1, n):
            for way in (0, 1):
                @pl.when(gets(way, step))
                def _():
                    arrived(m, way, step)

    def tp_copy(kind, source, target, d, peer):
        return pltpu.make_async_remote_copy(
            source, target, tp_send.at[kind, d], tp_recv.at[kind, d],
            device_id=(g, f, peer), device_id_type=MESH,
        )

    def token_copy(d):
        return tp_copy(0, tokens_ref, rows_all.at[t], d, lax.rem(t + d, tp))

    def out_copy(d):
        peer = lax.rem(t + d, tp)
        return tp_copy(1, partial_out.at[peer], heard_out.at[d - 1], d, peer)

    def first_copy(d):
        return tp_copy(2, first_all.at[t], first_all.at[t], d, lax.rem(t + d, tp))

    def down_copy(d):
        peer = lax.rem(t + d, tp)
        return tp_copy(3, partial_down.at[peer], heard_down.at[d - 1], d, peer)

    def square_copy(d):
        return tp_copy(4, squares.at[0], squares.at[d], d, lax.rem(t + d, tp))

    others = range(1, tp)
    for d in others:
        token_copy(d).start()
    launch(0)
    launch(1)
    locals_ = [pltpu.make_async_copy(tokens_ref, rows_all.at[t], local_sem.at[0])]
    for index, (w, held) in enumerate(weights + [(w_down_ref, g_down)]):
        locals_.append(pltpu.make_async_copy(w, held.at[f], local_sem.at[index + 1]))
    for copy in locals_:
        copy.start()
    for copy in locals_:
        copy.wait()
    for d in others:
        token_copy(d).wait_recv()

    def normalize(source, gain_ref):
        total = jnp.zeros((rows, 1), f32)
        for p in range(tp):
            values = source[p].astype(f32)
            total += jnp.sum(values * values, axis=1, keepdims=True)
        factor = lax.rsqrt(total / features + epsilon)
        for p in range(tp):
            part = pl.ds(p * width, width)
            scaled = source[p].astype(f32) * factor * gain_ref[:, part]
            normed[:, part] = scaled.astype(jnp.bfloat16)

    def accumulate(held, acc):
        depth = held.shape[1]
        acc[...] = jnp.zeros_like(acc)

        def step(j, carry):
            columns = pl.ds(pl.multiple_of(j * depth, 128), depth)
            acc[...] += jnp.dot(normed[:, columns], held[j], preferred_element_type=f32)
            return carry

        lax.fori_loop(0, n, step, 0)

    normalize(rows_all, attn_gain_ref)
    low_rank = jnp.dot(normed[...], w_low_ref[...], preferred_element_type=f32)
    lifted = jnp.dot(low_rank.astype(jnp.bfloat16), w_lift_ref[...], preferred_element_type=f32)
    log_decay[...] = jax.nn.log_sigmoid(lifted + decay_bias_ref[...]) / 16.0

    def pair(a, b, after):
        for step in range(1, n):
            tick(a, step)
            tick(b, step)
            if step == max(n - 2, 1):
                for m in after:
                    launch(m)

    pair(0, 1, (2, 3))
    all_arrived(0)
    mix_acc = up_acc.at[:, pl.ds(0, mix_rows.shape[1])]
    accumulate(g_mix, mix_acc)
    mix_rows[...] = mix_acc[...].astype(jnp.bfloat16)

    heads = mix_rows.shape[1] // (2 * DK + DV)
    at_row = lax.broadcasted_iota(jnp.int32, (BLOCK, BLOCK), 0)
    at_col = lax.broadcasted_iota(jnp.int32, (BLOCK, BLOCK), 1)
    causal = at_row >= at_col
    lower = causal.astype(f32)

    def dot(a, b, ca, cb):
        return lax.dot_general(
            a, b, (((ca,), (cb,)), ((), ())), precision=highest, preferred_element_type=f32
        )

    state[...] = jnp.zeros_like(state)

    def block_step(block, carry):
        here = pl.ds(pl.multiple_of(block * BLOCK, BLOCK), BLOCK)
        for h in range(heads):
            query = mix_rows[here, pl.ds(h * DK, DK)].astype(f32) * DK ** (-0.5)
            key = mix_rows[here, pl.ds((heads + h) * DK, DK)].astype(f32)
            value = mix_rows[here, pl.ds(2 * heads * DK + h * DV, DV)].astype(f32)
            cum = dot(lower, log_decay[here, pl.ds(h * DK, DK)], 1, 0)
            last = cum[BLOCK - 1 :, :]
            query_dec = query * jnp.exp(cum)
            key_dec = key * jnp.exp(-cum)
            scores = jnp.where(causal, dot(query_dec, key_dec, 1, 1), 0.0)
            held = state[h]
            out = dot(scores, value, 1, 0) + dot(query_dec, held, 1, 0)
            decay = jnp.transpose(jnp.broadcast_to(jnp.exp(last), (DK, DK)))
            decay = jnp.concatenate([decay] * (DV // DK), axis=1)
            state[h] = decay * held + dot(key * jnp.exp(last - cum), value, 0, 0)
            factor = lax.rsqrt(jnp.mean(out * out, axis=1, keepdims=True) + epsilon)
            mixed[here, pl.ds(h * DV, DV)] = (out * factor * head_gain_ref[...]).astype(jnp.bfloat16)
        return carry

    lax.fori_loop(0, rows // BLOCK, block_step, 0)
    if n > 2:
        tick(2, 1)
    all_arrived(1)

    def block_place(j, columns):
        return j * columns // width, pl.ds(pl.multiple_of(lax.rem(j * columns, width), 128), columns)

    def out_step(j, carry):
        p, part = block_place(j, g_out.shape[2])
        terms = jnp.dot(mixed[...], g_out[j], preferred_element_type=f32)
        partial_out[p, :, part] = terms.astype(jnp.bfloat16)
        return carry

    lax.fori_loop(0, n, out_step, 0)
    for d in others:
        out_copy(d).start()
    if n > 2:
        tick(3, 1)
    for d in others:
        out_copy(d).wait_recv()
    total = partial_out[t].astype(f32)
    for d in others:
        total += heard_out[d - 1].astype(f32)
    first_all[t] = (rows_all[t].astype(f32) + total).astype(jnp.bfloat16)
    for d in others:
        first_copy(d).start()
    for step in range(2, n - 1):
        tick(2, step)
        tick(3, step)
    launch(4)
    launch(5)
    for d in others:
        first_copy(d).wait_recv()
    normalize(first_all, ffn_gain_ref)
    tick(2, n - 1)
    all_arrived(2)
    accumulate(g_gate, gate_acc)
    tick(3, n - 1)
    tick(4, 1)
    all_arrived(3)
    accumulate(g_up, up_acc)
    gate = gate_acc[...]
    hidden[...] = (gate / (1.0 + jnp.exp(-gate)) * up_acc[...]).astype(jnp.bfloat16)
    eager = g_down.shape[2] == width

    def down_block(j):
        p, part = block_place(j, g_down.shape[2])
        terms = jnp.dot(hidden[...], g_down[j], preferred_element_type=f32)
        partial_down[p, :, part] = terms.astype(jnp.bfloat16)
        if eager:
            for d in others:
                @pl.when(j == lax.rem(t + d, tp))
                def _():
                    down_copy(d).start()

    down_block(f)
    for step in range(1, n):
        if step > 1:
            tick(4, step)
        tick(5, step)
        for way in (0, 1):
            @pl.when(gets(way, step))
            def _():
                arrived(4, way, step)
                arrived(5, way, step)
                down_block(f - step if way == 0 else f + step)
    if not eager:
        for d in others:
            down_copy(d).start()
    for d in others:
        down_copy(d).wait_recv()
    second = partial_down[t].astype(f32)
    for d in others:
        second += heard_down[d - 1].astype(f32)
    second = first_all[t].astype(f32) + second
    ones = jnp.ones((8, width), f32)
    squares[0] = dot(ones, second * second, 1, 1)
    for d in others:
        square_copy(d).start()
    for d in others:
        square_copy(d).wait_recv()
    whole = squares[0]
    for d in others:
        whole += squares[d]
    factor = lax.rsqrt(jnp.transpose(whole) / features + epsilon)[:, :1]
    result_ref[...] = (second * factor * final_gain_ref[...]).astype(jnp.bfloat16)

    for m in range(len(messages)):
        for step in range(1, n):
            for way in (0, 1):
                @pl.when(gives(way, step))
                def _():
                    z_copy(m, way, step).wait_send()

                @pl.when(gets(way, step))
                def _():
                    y_copy(m, way, step).wait_send()
    for d in others:
        for copy in (token_copy, out_copy, first_copy, down_copy, square_copy):
            copy(d).wait_send()


def body(
    sizes, tokens, attn_gain, w_query, w_key, w_value, w_low, w_lift, decay_bias, head_gain,
    w_out, ffn_gain, w_gate, w_up, w_down, final_gain,
):
    n, tp = sizes
    rows, width = tokens.shape
    w_mix = jnp.concatenate([w_query, w_key, w_value], axis=1)
    bf16, f32 = jnp.bfloat16, jnp.float32
    units, mix_width, keys = w_gate.shape[1], w_mix.shape[1], w_query.shape[1]
    values = w_value.shape[1]
    held = [pltpu.VMEM((n, *w.shape), bf16) for w in (w_mix, w_out, w_gate, w_up, w_down)]
    messages = 4 + DOWN_CHUNKS
    dma = pltpu.SemaphoreType.DMA
    anywhere = pl.BlockSpec(memory_space=pl.ANY)
    inside = pl.BlockSpec(memory_space=pltpu.VMEM)
    return pl.pallas_call(
        functools.partial(layer_kernel, sizes),
        name="layer",
        out_shape=jax.ShapeDtypeStruct((rows, width), bf16),
        in_specs=[anywhere] + [inside] * 7 + [anywhere] * 5,
        out_specs=inside,
        scratch_shapes=held + [
            pltpu.VMEM((tp, rows, width), bf16),
            pltpu.VMEM((rows, width * tp), bf16),
            pltpu.VMEM((rows, mix_width), bf16),
            pltpu.VMEM((rows, keys), f32),
            pltpu.VMEM((rows, values), bf16),
            pltpu.VMEM((keys // DK, DK, DV), f32),
            pltpu.VMEM((tp, rows, width), bf16),
            pltpu.VMEM((tp - 1, rows, width), bf16),
            pltpu.VMEM((tp, rows, width), bf16),
            pltpu.VMEM((rows, units), f32),
            pltpu.VMEM((rows, units), f32),
            pltpu.VMEM((rows, units), bf16),
            pltpu.VMEM((tp, rows, width), bf16),
            pltpu.VMEM((tp - 1, rows, width), bf16),
            pltpu.VMEM((tp, 8, rows), f32),
            dma((messages, 2, n)),
            dma((messages, 2, n)),
            dma((messages, 2, n)),
            dma((messages, 2, n)),
            dma((5, tp)),
            dma((5, tp)),
            dma((6,)),
        ],
        compiler_params=pltpu.CompilerParams(
            collective_id=0, has_side_effects=True, vmem_limit_bytes=63 * 1024 * 1024
        ),
    )(
        tokens, attn_gain[None], w_low, w_lift, decay_bias[None], head_gain[None],
        ffn_gain[None], final_gain[None], w_mix, w_out, w_gate, w_up, w_down,
    )


def solution(mesh):
    sizes = (mesh.shape["fs"], mesh.shape["tp"])
    return jax.shard_map(
        functools.partial(body, sizes),
        mesh=mesh,
        in_specs=(
            P(("grp", "fs"), "tp"),
            P(),
            P("fs", "tp"),
            P("fs", "tp"),
            P("fs", "tp"),
            P(),
            P(None, "tp"),
            P("tp"),
            P(),
            P("tp", "fs"),
            P(),
            P("fs", "tp"),
            P("fs", "tp"),
            P("tp", "fs"),
            P("tp"),
        ),
        out_specs=P(("grp", "fs"), "tp"),
        check_vma=False,
    )
```

time: 622 us -> 244 us (0.39)
  waiting for transfers between devices: 515 us -> 0 us
  Pallas kernels: 0 us -> 237 us
  matrix products: 43.5 us -> 0 us
  other arithmetic: 27.3 us -> 2.28 us
  between operations: 13.7 us -> 0.01 us
  local copies, waits for them, and re-layouts: 14.3 us -> 3.78 us
    all_gather x8 -> x0, waiting for transfers between devices: 432 us -> none  [the longest x1 107 us: body(): lax.all_gather(w_down, 'fs', axis=1, tiled=True)]
    pallas_call x0 -> x1, Pallas kernels: none -> 237 us  [body(): pl.pallas_call(functools.partial(layer_kernel, sizes), name='layer', out_...]
    psum x1 -> x0, waiting for transfers between devices: 47.8 us -> none  [body(): lax.psum(out_terms.astype(jnp.bfloat16), 'tp').astype(jnp.float32)]
    dot_general x11 -> x0, matrix products: 43.5 us -> none  [the longest x4 15.3 us: add_pieces(): jnp.dot(source, weight_piece, preferred_element_type=jnp.float32)]
    reduce_scatter x1 -> x0, waiting for transfers between devices: 29.6 us -> none  [body(): lax.psum_scatter(down_terms.astype(jnp.bfloat16), 'tp', scatter_dimension...]
    add x8 -> x0, other arithmetic: 8.52 us -> none  [advance(): return (decay_step[..., None] * carry_state + added, carry_state)]
    reduce_sum x3 -> x0, other arithmetic: 7.42 us -> none  [the longest x2 6.14 us: rms_rows(): jnp.mean(values * values, axis=-1, keepdims=True) + epsilon]
  transfers between devices with their start and end apart: 10 -> 0, of which waited for: 10 -> 0; matrix products, arithmetic and copies ran while one was open for 10% -> 0% of each run, Pallas kernels for 0% -> 0%
where the time goes in v1:
time: 244 us; the launch traced here: 243 us
  Pallas kernels  237 us (97%)
  local copies, waits for them, and re-layouts  3.78 us (2%)
    pallas_call x1, Pallas kernels, body(): pl.pallas_call(functools.partial(layer_kernel, sizes), name='layer', out_...  237 us

profile of v1, /device:TPU:0, one launch (start us, length us, event | category | flops | bytes accessed | tf_op | source)
XLA Modules:
  0.0 243.4 jit_solution(1269756042533368269)
XLA Ops:
  0.0 1.9 copy.16.w_low_ref
  1.9 2.3 pad_maximum_fusion.w_mix_ref
  4.2 237.4 %layer.1 = bf16[512,512]{1,0:T(8,128)(2,1)} custom-call(bf16[512,512]{1,0:T(8,128)(2,1)} %tokens_ref.1, f32[1,2048]{1,0:T(1,128)} %bitcast.5, bf16[2048,32]{1,0:T(8,128)(2,1)} %copy.16.w_low_ref, bf16[32,256]{1,0:T(8,128)(2,1)} %w_lift_ref.1, f32[1,256]{1,0:T(1,128)} %bitcast.8, f32[1,256]{1,0:T(1,128)} %bitcast.9, f32[1,2048]{1,0:T(1,128)} %bitcast.6, ...), custom_call_target="tpu_custom_call" | custom-call | tf_op jit(solution)/shard_map/layer/pallas_call | solution.py:382
  241.6 1.9 copy.18

commit v2 on v1

--- a/solution.py
+++ b/solution.py
@@ -13,7 +13,7 @@
 epsilon = 1e-06
 highest = lax.Precision.HIGHEST
 MESH = pl.DeviceIdType.MESH
-DOWN_CHUNKS = 2
+LANES = 128
 
 
 def layer_kernel(
@@ -26,7 +26,9 @@
     head_gain_ref,
     ffn_gain_ref,
     final_gain_ref,
-    w_mix_ref,
+    w_query_ref,
+    w_key_ref,
+    w_value_ref,
     w_out_ref,
     w_gate_ref,
     w_up_ref,
@@ -52,6 +54,8 @@
     partial_down,
     heard_down,
     squares,
+    down_send,
+    down_recv,
     z_send,
     z_recv,
     y_send,
@@ -66,9 +70,24 @@
     features = width * tp
     f32 = jnp.float32
 
-    weights = [(w_mix_ref, g_mix), (w_out_ref, g_out), (w_gate_ref, g_gate), (w_up_ref, g_up)]
-    messages = [(w, held, 0, 1) for w, held in weights]
-    messages += [(w_down_ref, g_down, c, DOWN_CHUNKS) for c in range(DOWN_CHUNKS)]
+    messages, owned = [], []
+    for group in (
+        ((w_query_ref, w_key_ref, w_value_ref), g_mix),
+        ((w_out_ref,), g_out),
+        ((w_gate_ref,), g_gate),
+        ((w_up_ref,), g_up),
+    ):
+        column = 0
+        for w in group[0]:
+            messages.append((w, group[1], 0, column, w.shape[1]))
+            owned.append(messages[-1])
+            column += w.shape[1]
+    chunks = w_down_ref.shape[1] // LANES
+    owned.append((w_down_ref, g_down, 0, 0, w_down_ref.shape[1]))
+    first_down = len(messages)
+    messages += [(w_down_ref, g_down, c * LANES, c * LANES, LANES) for c in range(chunks)]
+    opening, middle = range(4), range(4, first_down)
+    closing = range(first_down, len(messages))
 
     barrier = pltpu.get_barrier_semaphore()
 
@@ -87,17 +106,13 @@
     met = jnp.where(f > 0, 1, 0) + jnp.where(f < n - 1, 1, 0) + tp
     pl.semaphore_wait(barrier, met)
 
-    def span(m, group):
-        w, _, chunk, chunks = messages[m]
+    def z_copy(m, way, step):
+        w, held, start, column, columns = messages[m]
+        owner = f - (step - 1) if way == 0 else f + (step - 1)
         part = w.shape[0] // 2
-        length = part // chunks
-        return pl.ds(pl.multiple_of(group * part + chunk * length, 16), length)
-
-    def z_copy(m, way, step):
-        w, held, _, _ = messages[m]
-        owner = f - (step - 1) if way == 0 else f + (step - 1)
-        at = held.at[owner, span(m, g)]
-        source = w.at[span(m, g)] if step == 1 else at
+        half = pl.ds(pl.multiple_of(g * part, 16), part)
+        at = held.at[owner, half, pl.ds(column, columns)]
+        source = w.at[half, pl.ds(start, columns)] if step == 1 else at
         target = f + 1 if way == 0 else f - 1
         return pltpu.make_async_remote_copy(
             source, at, z_send.at[m, way, step], z_recv.at[m, way, step],
@@ -105,9 +120,10 @@
         )
 
     def y_copy(m, way, step):
-        held = messages[m][1]
-        owner = f - step if way == 0 else f + step
-        at = held.at[owner, span(m, g)]
+        w, held, _, column, columns = messages[m]
+        part = w.shape[0] // 2
+        half = pl.ds(pl.multiple_of(g * part, 16), part)
+        at = held.at[f + step * (2 * way - 1), half, pl.ds(column, columns)]
         return pltpu.make_async_remote_copy(
             at, at, y_send.at[m, way, step], y_recv.at[m, way, step],
             device_id=(1 - g, f, t), device_id_type=MESH,
@@ -165,23 +181,35 @@
     def first_copy(d):
         return tp_copy(2, first_all.at[t], first_all.at[t], d, lax.rem(t + d, tp))
 
-    def down_copy(d):
+    def down_copy(d, c):
         peer = lax.rem(t + d, tp)
-        return tp_copy(3, partial_down.at[peer], heard_down.at[d - 1], d, peer)
+        part = pl.ds(c * (width // chunks), width // chunks)
+        return pltpu.make_async_remote_copy(
+            partial_down.at[peer, :, part], heard_down.at[d - 1, :, part],
+            down_send.at[c, d], down_recv.at[c, d],
+            device_id=(g, f, peer), device_id_type=MESH,
+        )
 
     def square_copy(d):
-        return tp_copy(4, squares.at[0], squares.at[d], d, lax.rem(t + d, tp))
+        return tp_copy(3, squares.at[0], squares.at[d], d, lax.rem(t + d, tp))
 
     others = range(1, tp)
+    for m in opening:
+        launch(m)
     for d in others:
         token_copy(d).start()
-    launch(0)
-    launch(1)
     locals_ = [pltpu.make_async_copy(tokens_ref, rows_all.at[t], local_sem.at[0])]
-    for index, (w, held) in enumerate(weights + [(w_down_ref, g_down)]):
-        locals_.append(pltpu.make_async_copy(w, held.at[f], local_sem.at[index + 1]))
+    for index, (w, held, _, column, columns) in enumerate(owned):
+        at = held.at[f, :, pl.ds(column, columns)]
+        locals_.append(pltpu.make_async_copy(w, at, local_sem.at[index + 1]))
     for copy in locals_:
         copy.start()
+
+    for step in range(1, max(n - 1, 2)):
+        for m in opening:
+            tick(m, step)
+    for m in middle:
+        launch(m)
     for copy in locals_:
         copy.wait()
     for d in others:
@@ -210,20 +238,17 @@
         lax.fori_loop(0, n, step, 0)
 
     normalize(rows_all, attn_gain_ref)
-    low_rank = jnp.dot(normed[...], w_low_ref[...], preferred_element_type=f32)
+    low_rank = lax.dot_general(
+        normed[...], w_low_ref[...], (((1,), (1,)), ((), ())), preferred_element_type=f32
+    )
     lifted = jnp.dot(low_rank.astype(jnp.bfloat16), w_lift_ref[...], preferred_element_type=f32)
     log_decay[...] = jax.nn.log_sigmoid(lifted + decay_bias_ref[...]) / 16.0
 
-    def pair(a, b, after):
-        for step in range(1, n):
-            tick(a, step)
-            tick(b, step)
-            if step == max(n - 2, 1):
-                for m in after:
-                    launch(m)
-
-    pair(0, 1, (2, 3))
-    all_arrived(0)
+    if n > 2:
+        for m in opening:
+            tick(m, n - 1)
+    for m in range(3):
+        all_arrived(m)
     mix_acc = up_acc.at[:, pl.ds(0, mix_rows.shape[1])]
     accumulate(g_mix, mix_acc)
     mix_rows[...] = mix_acc[...].astype(jnp.bfloat16)
@@ -262,9 +287,10 @@
         return carry
 
     lax.fori_loop(0, rows // BLOCK, block_step, 0)
+    gate_at, up_at = middle
     if n > 2:
-        tick(2, 1)
-    all_arrived(1)
+        tick(gate_at, 1)
+    all_arrived(3)
 
     def block_place(j, columns):
         return j * columns // width, pl.ds(pl.multiple_of(lax.rem(j * columns, width), 128), columns)
@@ -279,7 +305,7 @@
     for d in others:
         out_copy(d).start()
     if n > 2:
-        tick(3, 1)
+        tick(up_at, 1)
     for d in others:
         out_copy(d).wait_recv()
     total = partial_out[t].astype(f32)
@@ -289,50 +315,62 @@
     for d in others:
         first_copy(d).start()
     for step in range(2, n - 1):
-        tick(2, step)
-        tick(3, step)
-    launch(4)
-    launch(5)
+        tick(gate_at, step)
+        tick(up_at, step)
+    for m in closing:
+        launch(m)
     for d in others:
         first_copy(d).wait_recv()
     normalize(first_all, ffn_gain_ref)
-    tick(2, n - 1)
-    all_arrived(2)
+    tick(gate_at, n - 1)
+    all_arrived(gate_at)
     accumulate(g_gate, gate_acc)
-    tick(3, n - 1)
-    tick(4, 1)
-    all_arrived(3)
+    tick(up_at, n - 1)
+    for m in closing:
+        tick(m, 1)
+    all_arrived(up_at)
     accumulate(g_up, up_acc)
     gate = gate_acc[...]
     hidden[...] = (gate / (1.0 + jnp.exp(-gate)) * up_acc[...]).astype(jnp.bfloat16)
     eager = g_down.shape[2] == width
 
-    def down_block(j):
-        p, part = block_place(j, g_down.shape[2])
-        terms = jnp.dot(hidden[...], g_down[j], preferred_element_type=f32)
+    def down_block(j, c):
+        place = j * g_down.shape[2] + c * LANES
+        p, part = place // width, pl.ds(pl.multiple_of(lax.rem(place, width), LANES), LANES)
+        columns = pl.ds(c * LANES, LANES)
+        terms = jnp.dot(hidden[...], g_down[j, :, columns], preferred_element_type=f32)
         partial_down[p, :, part] = terms.astype(jnp.bfloat16)
         if eager:
             for d in others:
                 @pl.when(j == lax.rem(t + d, tp))
                 def _():
-                    down_copy(d).start()
-
-    down_block(f)
+                    down_copy(d, c).start()
+
+    for c in range(chunks):
+        down_block(f, c)
     for step in range(1, n):
         if step > 1:
-            tick(4, step)
-        tick(5, step)
-        for way in (0, 1):
-            @pl.when(gets(way, step))
-            def _():
-                arrived(4, way, step)
-                arrived(5, way, step)
-                down_block(f - step if way == 0 else f + step)
+            for m in closing:
+                tick(m, step)
+        for c, m in enumerate(closing):
+            def from_way(way, carry):
+                j = f + step * (2 * way - 1)
+
+                @pl.when(jnp.logical_and(j >= 0, j < n))
+                def _():
+                    y_copy(m, way, step).wait_recv()
+                    down_block(j, c)
+
+                return carry
+
+            lax.fori_loop(0, 2, from_way, 0)
     if not eager:
         for d in others:
-            down_copy(d).start()
-    for d in others:
-        down_copy(d).wait_recv()
+            for c in range(chunks):
+                down_copy(d, c).start()
+    for d in others:
+        for c in range(chunks):
+            down_copy(d, c).wait_recv()
     second = partial_down[t].astype(f32)
     for d in others:
         second += heard_down[d - 1].astype(f32)
@@ -360,8 +398,10 @@
                 def _():
                     y_copy(m, way, step).wait_send()
     for d in others:
-        for copy in (token_copy, out_copy, first_copy, down_copy, square_copy):
+        for copy in (token_copy, out_copy, first_copy, square_copy):
             copy(d).wait_send()
+        for c in range(chunks):
+            down_copy(d, c).wait_send()
 
 
 def body(
@@ -370,12 +410,13 @@
 ):
     n, tp = sizes
     rows, width = tokens.shape
-    w_mix = jnp.concatenate([w_query, w_key, w_value], axis=1)
     bf16, f32 = jnp.bfloat16, jnp.float32
-    units, mix_width, keys = w_gate.shape[1], w_mix.shape[1], w_query.shape[1]
-    values = w_value.shape[1]
-    held = [pltpu.VMEM((n, *w.shape), bf16) for w in (w_mix, w_out, w_gate, w_up, w_down)]
-    messages = 4 + DOWN_CHUNKS
+    units, keys, values = w_gate.shape[1], w_query.shape[1], w_value.shape[1]
+    mix_width = 2 * keys + values
+    held = [pltpu.VMEM((n, w_query.shape[0], mix_width), bf16)]
+    held += [pltpu.VMEM((n, *w.shape), bf16) for w in (w_out, w_gate, w_up, w_down)]
+    chunks = w_down.shape[1] // LANES
+    messages = 6 + chunks
     dma = pltpu.SemaphoreType.DMA
     anywhere = pl.BlockSpec(memory_space=pl.ANY)
     inside = pl.BlockSpec(memory_space=pltpu.VMEM)
@@ -383,7 +424,7 @@
         functools.partial(layer_kernel, sizes),
         name="layer",
         out_shape=jax.ShapeDtypeStruct((rows, width), bf16),
-        in_specs=[anywhere] + [inside] * 7 + [anywhere] * 5,
+        in_specs=[anywhere] + [inside] * 7 + [anywhere] * 7,
         out_specs=inside,
         scratch_shapes=held + [
             pltpu.VMEM((tp, rows, width), bf16),
@@ -401,20 +442,22 @@
             pltpu.VMEM((tp, rows, width), bf16),
             pltpu.VMEM((tp - 1, rows, width), bf16),
             pltpu.VMEM((tp, 8, rows), f32),
+            dma((chunks, tp)),
+            dma((chunks, tp)),
             dma((messages, 2, n)),
             dma((messages, 2, n)),
             dma((messages, 2, n)),
             dma((messages, 2, n)),
-            dma((5, tp)),
-            dma((5, tp)),
-            dma((6,)),
+            dma((4, tp)),
+            dma((4, tp)),
+            dma((8,)),
         ],
         compiler_params=pltpu.CompilerParams(
             collective_id=0, has_side_effects=True, vmem_limit_bytes=63 * 1024 * 1024
         ),
     )(
-        tokens, attn_gain[None], w_low, w_lift, decay_bias[None], head_gain[None],
-        ffn_gain[None], final_gain[None], w_mix, w_out, w_gate, w_up, w_down,
+        tokens, attn_gain[None], w_low.T, w_lift, decay_bias[None], head_gain[None],
+        ffn_gain[None], final_gain[None], w_query, w_key, w_value, w_out, w_gate, w_up, w_down,
     )
 
 

time: 244 us -> 232 us (0.951)
  Pallas kernels: 237 us -> 230 us
    pallas_call x1, Pallas kernels: 237 us -> 230 us  [body(): pl.pallas_call(functools.partial(layer_kernel, sizes), name='layer', out_...]
where the time goes in v2:
time: 232 us
  Pallas kernels  230 us (99%)
    pallas_call x1, Pallas kernels, body(): pl.pallas_call(functools.partial(layer_kernel, sizes), name='layer', out_...  230 us

profile of v2, /device:TPU:0, one launch (start us, length us, event | category | flops | bytes accessed | tf_op | source)
XLA Modules:
  0.0 232.3 jit_solution(14780415520039533191)
XLA Ops:
  0.0 230.4 %layer.1 = bf16[512,512]{1,0:T(8,128)(2,1)} custom-call(bf16[512,512]{1,0:T(8,128)(2,1)} %tokens_ref.1, f32[1,2048]{1,0:T(1,128)} %bitcast.7, bf16[32,2048]{1,0:T(8,128)(2,1)} %bitcast.6, bf16[32,256]{1,0:T(8,128)(2,1)} %w_lift_ref.1, f32[1,256]{1,0:T(1,128)} %bitcast.10, f32[1,256]{1,0:T(1,128)} %bitcast.11, f32[1,2048]{1,0:T(1,128)} %bitcast.8, ...), custom_call_target="tpu_custom_call" | custom-call | tf_op jit(solution)/shard_map/layer/pallas_call | solution.py:423
  230.4 1.9 copy.17

commit v3 on v2

--- a/solution.py
+++ b/solution.py
@@ -286,10 +286,12 @@
             mixed[here, pl.ds(h * DV, DV)] = (out * factor * head_gain_ref[...]).astype(jnp.bfloat16)
         return carry
 
-    lax.fori_loop(0, rows // BLOCK, block_step, 0)
     gate_at, up_at = middle
+    blocks = rows // BLOCK
+    lax.fori_loop(0, blocks // 2, block_step, 0)
     if n > 2:
         tick(gate_at, 1)
+    lax.fori_loop(blocks // 2, blocks, block_step, 0)
     all_arrived(3)
 
     def block_place(j, columns):
@@ -306,6 +308,8 @@
         out_copy(d).start()
     if n > 2:
         tick(up_at, 1)
+    if n > 3:
+        tick(gate_at, 2)
     for d in others:
         out_copy(d).wait_recv()
     total = partial_out[t].astype(f32)
@@ -315,7 +319,8 @@
     for d in others:
         first_copy(d).start()
     for step in range(2, n - 1):
-        tick(gate_at, step)
+        if step > 2:
+            tick(gate_at, step)
         tick(up_at, step)
     for m in closing:
         launch(m)

time: 232 us -> 232 us (level)
  no operation moved by 1% of the time
where the time goes in v3:
time: 232 us
  Pallas kernels  230 us (99%)
    pallas_call x1, Pallas kernels, body(): pl.pallas_call(functools.partial(layer_kernel, sizes), name='layer', out_...  230 us

profile of v3, /device:TPU:0, one launch (start us, length us, event | category | flops | bytes accessed | tf_op | source)
XLA Modules:
  0.0 232.3 jit_solution(6496554131433043323)
XLA Ops:
  0.0 230.4 %layer.1 = bf16[512,512]{1,0:T(8,128)(2,1)} custom-call(bf16[512,512]{1,0:T(8,128)(2,1)} %tokens_ref.1, f32[1,2048]{1,0:T(1,128)} %bitcast.7, bf16[32,2048]{1,0:T(8,128)(2,1)} %bitcast.6, bf16[32,256]{1,0:T(8,128)(2,1)} %w_lift_ref.1, f32[1,256]{1,0:T(1,128)} %bitcast.10, f32[1,256]{1,0:T(1,128)} %bitcast.11, f32[1,2048]{1,0:T(1,128)} %bitcast.8, ...), custom_call_target="tpu_custom_call" | custom-call | tf_op jit(solution)/shard_map/layer/pallas_call | solution.py:428
  230.4 1.9 copy.17
